TPU v7x, 32 devices: a whole 2x2x4 slice. The times are simulated.
32 devices in a mesh: grp: 2 (over y), sp: 4 (over z), dp: 4 (over x, core).
Axes of the slice: x: 2, y: 2, z: 4, core: 2. Of those that a mesh axis runs over, the one named last changes fastest.
Arguments:
- query_rows: bfloat16 [8, 512, 2048], P(('grp', 'dp'), 'sp'), parts along dimension 0, may hold values from -6 to 6
- key_rows: bfloat16 [8, 512, 2048], P(('grp', 'dp'), 'sp'), parts along dimension 0, may hold values from -6 to 6
- value_rows: bfloat16 [8, 512, 2048], P(('grp', 'dp'), 'sp'), parts along dimension 0, may hold values from -6 to 6
- query_gain: float32 [64], replicated, may hold values from 1.1 to 7
- key_gain: float32 [64], replicated, may hold values from 1.1 to 7
- lambdas: float32 [16], replicated, may hold values from 0.3 to 0.8
- head_gain: float32 [128], replicated, may hold values from 0.1 to 1.9
- out_weight: bfloat16 [2048, 2048], P(None, 'dp'), may hold values from -0.125 to 0.125
Outputs:
- attended: bfloat16 [8, 512, 2048], P(('grp', 'dp'), 'sp'), parts along dimension 0
There are 2 independent parts, one for each index of `grp`. A program takes and returns all parts, laid end to end along the dimension named above; an argument that names none is the same for every part. Nothing has to cross between parts.
All inputs are finite; a program needn't handle non-finite values.
Results may differ from a plain program's by a relative error of at most 0.008.
The roundings to bfloat16 on the way count: a program that leaves them out, or rounds other values in their place, can miss the bound.
Values may be sent and summed in bfloat16 or wider, within the bound.
A program may use at most 128 MiB of HBM per device.

v0:
```python
import jax
import jax.numpy as jnp
from jax import lax
from jax.sharding import PartitionSpec as P

EPSILON = 1e-06
OUT_SCALE = 0.8


def norm_rotate(field_rows, gain_vector, positions):
    widened = field_rows.astype(jnp.float32)
    normed = (
        widened
        * lax.rsqrt(jnp.mean(widened * widened, axis=-1, keepdims=True) + EPSILON)
        * gain_vector
    )
    half_size = field_rows.shape[-1] // 2
    inverse = 10000.0 ** (-jnp.arange(half_size, dtype=jnp.float32) / half_size)
    angles = (positions[:, None] * inverse[None, :]).reshape(positions.shape[0], 1, 1, half_size)
    cosine_part = jnp.cos(angles)
    sine_part = jnp.sin(angles)
    first_half = normed[..., :half_size]
    second_half = normed[..., half_size:]
    turned = jnp.concatenate(
        [
            first_half * cosine_part - second_half * sine_part,
            second_half * cosine_part + first_half * sine_part,
        ],
        axis=-1,
    )
    return turned.astype(jnp.bfloat16)


def head_norm(raw_heads, gain_vector):
    scaled = raw_heads * lax.rsqrt(
        jnp.mean(raw_heads * raw_heads, axis=-1, keepdims=True) + EPSILON
    )
    return (scaled * gain_vector * OUT_SCALE).astype(jnp.bfloat16)


def block_size():
    return 512


def attend(query_head, key_head, value_head, weight_two, gain_vector):
    length = query_head.shape[0]
    block_rows = block_size()
    score_scale = query_head.shape[-1] ** (-0.5)
    offsets = jnp.arange(block_rows, dtype=jnp.int32)
    value_size = value_head.shape[-1]

    def one_block(number):
        first_row = number * block_rows
        query_block = lax.dynamic_slice_in_dim(query_head, first_row, block_rows, 0)
        query_positions = first_row + offsets

        def fill_scores(kblock, buffer):
            key_block = lax.dynamic_slice_in_dim(key_head, kblock * block_rows, block_rows, 0)
            scores = (
                jnp.einsum(
                    "qcd,kcd->cqk", query_block, key_block, preferred_element_type=jnp.float32
                )
                * score_scale
            )
            visible = (kblock * block_rows + offsets)[None, :] <= query_positions[:, None]
            scores = jnp.where(visible[None], scores, -1e30)
            return lax.dynamic_update_slice_in_dim(buffer, scores, kblock * block_rows, 2)

        start_buffer = jnp.full((2, block_rows, length), -1e30, jnp.float32)
        stored = lax.fori_loop(0, number + 1, fill_scores, start_buffer)
        highest = jnp.max(stored, axis=-1)
        totals = jnp.sum(jnp.exp(stored - highest[..., None]), axis=-1)

        def weigh_values(kblock, accumulated):
            scores = lax.dynamic_slice_in_dim(stored, kblock * block_rows, block_rows, 2)
            probabilities = jnp.exp(scores - highest[..., None]) / totals[..., None]
            mixing = (probabilities[0] - weight_two * probabilities[1]).astype(jnp.bfloat16)
            value_block = lax.dynamic_slice_in_dim(value_head, kblock * block_rows, block_rows, 0)
            return accumulated + jnp.dot(mixing, value_block, preferred_element_type=jnp.float32)

        return lax.fori_loop(
            0, number + 1, weigh_values, jnp.zeros((block_rows, value_size), jnp.float32)
        )

    blocks = lax.map(one_block, jnp.arange(length // block_rows, dtype=jnp.int32))
    return head_norm(blocks.reshape(length, value_size), gain_vector)


def local(query_rows, key_rows, value_rows, query_gain, key_gain, lambdas, head_gain, out_weight):
    tok_count = query_rows.shape[1]
    group_size = lax.axis_size("sp")
    head_size = query_gain.shape[0]
    value_size = head_gain.shape[0]
    heads_total = lambdas.shape[0]
    local_heads = heads_total // group_size

    def by_peer(tensor):
        return tensor.reshape(1, tok_count, group_size, tensor.shape[2] // group_size)

    query_in, key_in, value_in = (
        lax.all_to_all(by_peer(query_rows), "sp", split_axis=2, concat_axis=1, tiled=True),
        lax.all_to_all(by_peer(key_rows), "sp", split_axis=2, concat_axis=1, tiled=True),
        lax.all_to_all(by_peer(value_rows), "sp", split_axis=2, concat_axis=1, tiled=True),
    )
    length = tok_count * group_size
    positions = jnp.arange(length, dtype=jnp.float32)
    query_rot = norm_rotate(
        query_in.reshape(length, local_heads, 2, head_size), query_gain, positions
    )
    key_rot = norm_rotate(key_in.reshape(length, local_heads, 2, head_size), key_gain, positions)
    value_heads = value_in.reshape(length, local_heads, value_size)
    local_lambdas = lax.dynamic_slice_in_dim(
        lambdas, lax.axis_index("sp") * local_heads, local_heads
    )

    def per_head(head_index):
        return attend(
            query_rot[:, head_index],
            key_rot[:, head_index],
            value_heads[:, head_index],
            local_lambdas[head_index],
            head_gain,
        )

    outputs = lax.map(per_head, jnp.arange(local_heads, dtype=jnp.int32))
    outputs = jnp.transpose(outputs, (1, 0, 2)).reshape(1, length, 1, local_heads * value_size)
    returned = lax.all_to_all(outputs, "sp", split_axis=1, concat_axis=2, tiled=True)
    heads_rows = returned.reshape(tok_count, heads_total * value_size)
    attended = jnp.dot(
        heads_rows,
        lax.all_gather(out_weight, "dp", axis=1, tiled=True),
        preferred_element_type=jnp.float32,
    )
    return attended.astype(jnp.bfloat16).reshape(1, tok_count, attended.shape[1])


def solution(mesh):
    placed = (
        P(("grp", "dp"), "sp", None),
        P(("grp", "dp"), "sp", None),
        P(("grp", "dp"), "sp", None),
        P(),
        P(),
        P(),
        P(),
        P(None, "dp"),
    )
    return jax.shard_map(
        local, mesh=mesh, in_specs=placed, out_specs=P(("grp", "dp"), "sp", None), check_vma=False
    )
```

profile of v0, /device:TPU:0, one launch (start us, length us, event | category | flops | bytes accessed | tf_op | source)
XLA Modules:
  0.0 130.4 jit_solution(3775947803156317788)
XLA Ops:
  6.5 0.7 all-gather.2.cloned.1.call-update
  7.3 0.3 copy-done.1
  7.6 1.0 copy.25
  8.6 6.3 %all-to-all-start = ((bf16[1,128,4,512]{1,3,0,2:T(8,128)(2,1)}), bf16[1,128,4,512]{1,3,0,2:T(8,128)(2,1)S(1)}, u32[]{:S(2)}, u32[]{:S(2)}) async-start(bf16[1,128,4,512]{1,3,0,2:T(8,128)(2,1)} %bitcast.7), calls=%async_computation | async-start | bytes 1048576 | tf_op jit(solution)/shard_map/all_to_all | solution.py:102
  15.0 1.0 copy.27
  16.0 13.5 %all-to-all-done = bf16[1,128,4,512]{1,3,0,2:T(8,128)(2,1)S(1)} async-done(((bf16[1,128,4,512]{1,3,0,2:T(8,128)(2,1)}), bf16[1,128,4,512]{1,3,0,2:T(8,128)(2,1)S(1)}, u32[]{:S(2)}, u32[]{:S(2)}) %all-to-all-start) | async-done | bytes 524320 | tf_op jit(solution)/shard_map/all_to_all | solution.py:102
  29.5 3.6 %all-to-all-start.1 = ((bf16[1,128,4,512]{1,3,0,2:T(8,128)(2,1)}), bf16[1,128,4,512]{1,3,0,2:T(8,128)(2,1)S(1)}, u32[]{:S(2)}, u32[]{:S(2)}) async-start(bf16[1,128,4,512]{1,3,0,2:T(8,128)(2,1)} %bitcast.10), calls=%async_computation.1 | async-start | bytes 1048576 | tf_op jit(solution)/shard_map/all_to_all | solution.py:101
  33.1 0.3 copy.29
  33.4 1.1 copy.30
  34.4 12.7 %all-to-all-done.1 = bf16[1,128,4,512]{1,3,0,2:T(8,128)(2,1)S(1)} async-done(((bf16[1,128,4,512]{1,3,0,2:T(8,128)(2,1)}), bf16[1,128,4,512]{1,3,0,2:T(8,128)(2,1)S(1)}, u32[]{:S(2)}, u32[]{:S(2)}) %all-to-all-start.1) | async-done | bytes 524320 | tf_op jit(solution)/shard_map/all_to_all | solution.py:101
  47.1 4.1 %all-to-all-start.2 = ((bf16[1,128,4,512]{3,1,0,2:T(8,128)(2,1)}), bf16[1,128,4,512]{3,1,0,2:T(8,128)(2,1)}, u32[]{:S(2)}, u32[]{:S(2)}) async-start(bf16[1,128,4,512]{3,1,0,2:T(8,128)(2,1)} %copy.30), calls=%async_computation.2 | async-start | bytes 1048576 | tf_op jit(solution)/shard_map/all_to_all | solution.py:103
  51.3 0.1 dynamic_slice.42
  51.3 0.3 fusion.40
  51.7 0.7 copy.26
  52.4 0.4 reshape.151
  52.8 0.1 convert_bitcast_fusion
  52.9 0.7 copy.28
  53.6 0.4 reshape.152
  54.0 11.3 %all-to-all-done.2 = bf16[1,128,4,512]{3,1,0,2:T(8,128)(2,1)} async-done(((bf16[1,128,4,512]{3,1,0,2:T(8,128)(2,1)}), bf16[1,128,4,512]{3,1,0,2:T(8,128)(2,1)}, u32[]{:S(2)}, u32[]{:S(2)}) %all-to-all-start.2) | async-done | bytes 524320 | tf_op jit(solution)/shard_map/all_to_all | solution.py:103
  65.3 1.2 reshape.147
  66.6 0.1 multiply_reduce_fusion.2
  66.8 0.1 multiply_reduce_fusion.1
  67.0 0.3 multiply_multiply_fusion.1
  67.2 0.3 multiply_multiply_fusion
  67.5 0.3 subtract_convert_fusion
  67.9 1.1 pad_maximum_fusion
  69.0 26.1 %while.54 = (s32[]{:T(128)}, bf16[4,512,128]{1,2,0:T(8,128)(2,1)S(1)}, s32[4]{0:T(128)S(1)}, bf16[512,4,2,64]{0,3,2,1:T(8,128)(2,1)}, bf16[512,4,2,64]{0,3,2,1:T...) while((s32[]{:T(128)}, ...), condition=%wide.region_8.9_spmd, body=%wide.region_2.8_spmd.sunk | while | flops 138281984 | bytes 9979571 | solution.py:125
  69.0 0.6 dynamic_slice.79
  71.5 0.1 iota_compare_fusion.2
  71.6 2.0 %fusion.54 = (f32[2,512]{1,0:T(2,128)S(1)}, f32[2,512,512]{1,2,0:T(8,128)S(1)}) fusion(pred[512,512]{0,1:T(8,128)(4,1)S(1)} %iota_compare_fusion.2, bf16[512,4,2,64]{0,3,2,1:T(8,128)(2,1)} %get-tuple-element.419, s32[]{:T(128)S(6)} %select_n.36, bf16[512,4,2,64]{0,3,2,1:T(8,128)(2,1)} %get-tuple-element.420), kind=kOutput, calls=%fused_computation.57.clone.1 | convolution fusion | flops 69206528 | bytes 2626560 | tf_op jit(solution)/shard_map/while/body/eval_jaxpr/while/body/eval_jaxpr/sub | solution.py:72
  73.6 0.3 broadcast_divide_fusion.2
  73.9 0.6 dynamic_slice.80
  74.4 0.9 multiply_reduce_fusion.4
  75.4 0.1 fusion.55
  75.5 0.6 dynamic_slice.79
  78.0 0.1 iota_compare_fusion.2
  78.1 2.0 %fusion.54 = (f32[2,512]{1,0:T(2,128)S(1)}, f32[2,512,512]{1,2,0:T(8,128)S(1)}) fusion(pred[512,512]{0,1:T(8,128)(4,1)S(1)} %iota_compare_fusion.2, bf16[512,4,2,64]{0,3,2,1:T(8,128)(2,1)} %get-tuple-element.419, s32[]{:T(128)S(6)} %select_n.36, bf16[512,4,2,64]{0,3,2,1:T(8,128)(2,1)} %get-tuple-element.420), kind=kOutput, calls=%fused_computation.57.clone.1 | convolution fusion | flops 69206528 | bytes 2626560 | tf_op jit(solution)/shard_map/while/body/eval_jaxpr/while/body/eval_jaxpr/sub | solution.py:72
  80.1 0.3 broadcast_divide_fusion.2
  80.4 0.6 dynamic_slice.80
  81.0 0.9 multiply_reduce_fusion.4
  81.9 0.1 fusion.55
  82.0 0.6 dynamic_slice.79
  84.6 0.1 iota_compare_fusion.2
  84.7 2.0 %fusion.54 = (f32[2,512]{1,0:T(2,128)S(1)}, f32[2,512,512]{1,2,0:T(8,128)S(1)}) fusion(pred[512,512]{0,1:T(8,128)(4,1)S(1)} %iota_compare_fusion.2, bf16[512,4,2,64]{0,3,2,1:T(8,128)(2,1)} %get-tuple-element.419, s32[]{:T(128)S(6)} %select_n.36, bf16[512,4,2,64]{0,3,2,1:T(8,128)(2,1)} %get-tuple-element.420), kind=kOutput, calls=%fused_computation.57.clone.1 | convolution fusion | flops 69206528 | bytes 2626560 | tf_op jit(solution)/shard_map/while/body/eval_jaxpr/while/body/eval_jaxpr/sub | solution.py:72
  86.6 0.3 broadcast_divide_fusion.2
  86.9 0.6 dynamic_slice.80
  87.5 0.9 multiply_reduce_fusion.4
  88.4 0.1 fusion.55
  88.6 0.6 dynamic_slice.79
  91.1 0.1 iota_compare_fusion.2
  91.2 2.0 %fusion.54 = (f32[2,512]{1,0:T(2,128)S(1)}, f32[2,512,512]{1,2,0:T(8,128)S(1)}) fusion(pred[512,512]{0,1:T(8,128)(4,1)S(1)} %iota_compare_fusion.2, bf16[512,4,2,64]{0,3,2,1:T(8,128)(2,1)} %get-tuple-element.419, s32[]{:T(128)S(6)} %select_n.36, bf16[512,4,2,64]{0,3,2,1:T(8,128)(2,1)} %get-tuple-element.420), kind=kOutput, calls=%fused_computation.57.clone.1 | convolution fusion | flops 69206528 | bytes 2626560 | tf_op jit(solution)/shard_map/while/body/eval_jaxpr/while/body/eval_jaxpr/sub | solution.py:72
  93.1 0.3 broadcast_divide_fusion.2
  93.4 0.6 dynamic_slice.80
  94.0 0.9 multiply_reduce_fusion.4
  95.0 0.1 fusion.55
  95.1 0.9 copy.32
  96.0 0.5 broadcast.175
  96.5 3.8 %reduce = bf16[512,512]{1,0:T(8,128)(2,1)S(1)} reduce(bf16[512,1,1,512]{3,2,1,0:T(2,128)(2,1)S(1)} %bitcast.87, bf16[]{:T(256)} %broadcast.175), dimensions={1,2}, to_apply=%bitcast.59.reduce_sub_computation | reduce | bytes 1048578
  100.3 0.4 reshape.155
  100.7 16.4 %all_to_all.48 = bf16[4,2,32768]{2,1,0:T(2,128)(2,1)S(1)} all-to-all(bf16[4,2,32768]{2,1,0:T(2,128)(2,1)S(1)} %reshape.155), channel_id=1, replica_groups=mesh['grp'=2,'sp'=4,'dp'=4] {'sp'}, dimensions={0} | all-to-all | bytes 1048576 | tf_op jit(solution)/shard_map/all_to_all | solution.py:127
  117.1 0.5 reshape.156
  117.7 0.1 copy.34
  117.8 0.3 copy.33
  118.1 5.5 %fusion.38 = bf16[1,128,2048]{2,1,0:T(8,128)(2,1)} fusion(bf16[128,2048]{0,1:T(8,128)(2,1)S(1)} %bitcast.85, bf16[2048,2048]{1,0:T(8,128)(2,1)} %all-gather.2.cloned.1.call-done), kind=kOutput, calls=%fused_computation.38 | convolution fusion | flops 1074003968 | bytes 9437184 | tf_op jit(solution)/shard_map/dot_general | solution.py:129
  (28 shorter events, 0.3 us)
Async XLA Ops:
  6.5 1.0 copy-start.1
  6.5 8.4 %copy-start.2 = (bf16[1,128,2048]{2,1,0:T(8,128)(2,1)S(1)}, bf16[1,128,2048]{2,1,0:T(8,128)(2,1)}, u32[]{:S(2)}) copy-start(bf16[1,128,2048]{2,1,0:T(8,128)(2,1)} %param.12) | copy-start | bytes 1572868
  6.5 111.5 %all-gather.2.cloned.1.call-start = ((), (), s32[]{:S(2)}) async-start(), calls=%async_computation.4 | async-start | bytes 10485760 | tf_op jit(solution)/shard_map/all_gather | solution.py:131
  7.6 25.5 %copy-start.3 = (bf16[1,128,2048]{2,1,0:T(8,128)(2,1)S(1)}, bf16[1,128,2048]{2,1,0:T(8,128)(2,1)}, u32[]{:S(2)}) copy-start(bf16[1,128,2048]{2,1,0:T(8,128)(2,1)} %param.14) | copy-start | bytes 1572868
  8.6 20.8 %all-to-all-start = ((bf16[1,128,4,512]{1,3,0,2:T(8,128)(2,1)}), bf16[1,128,4,512]{1,3,0,2:T(8,128)(2,1)S(1)}, u32[]{:S(2)}, u32[]{:S(2)}) async-start(bf16[1,128,4,512]{1,3,0,2:T(8,128)(2,1)} %bitcast.7), calls=%async_computation | async-start | bytes 1048576 | tf_op jit(solution)/shard_map/all_to_all | solution.py:102
  29.5 21.8 %copy-start.7 = (f32[16]{0:T(128)S(1)}, f32[16]{0:T(128)}, u32[]{:S(2)}) copy-start(f32[16]{0:T(128)} %param.17) | copy-start | bytes 196
  29.5 17.6 %all-to-all-start.1 = ((bf16[1,128,4,512]{1,3,0,2:T(8,128)(2,1)}), bf16[1,128,4,512]{1,3,0,2:T(8,128)(2,1)S(1)}, u32[]{:S(2)}, u32[]{:S(2)}) async-start(bf16[1,128,4,512]{1,3,0,2:T(8,128)(2,1)} %bitcast.10), calls=%async_computation.1 | async-start | bytes 1048576 | tf_op jit(solution)/shard_map/all_to_all | solution.py:101
  47.1 18.2 %all-to-all-start.2 = ((bf16[1,128,4,512]{3,1,0,2:T(8,128)(2,1)}), bf16[1,128,4,512]{3,1,0,2:T(8,128)(2,1)}, u32[]{:S(2)}, u32[]{:S(2)}) async-start(bf16[1,128,4,512]{3,1,0,2:T(8,128)(2,1)} %copy.30), calls=%async_computation.2 | async-start | bytes 1048576 | tf_op jit(solution)/shard_map/all_to_all | solution.py:103
  65.3 1.6 %copy-start.5 = (f32[64]{0:T(128)S(1)}, f32[64]{0:T(128)}, u32[]{:S(2)}) copy-start(f32[64]{0:T(128)} %param.16) | copy-start | bytes 772
  66.6 0.7 copy-start.6
  67.5 1.5 %copy-start = (bf16[4,512,128]{1,2,0:T(8,128)(2,1)S(1)}, bf16[4,512,128]{1,2,0:T(8,128)(2,1)}, u32[]{:S(2)}) copy-start(bf16[4,512,128]{1,2,0:T(8,128)(2,1)} %custom-call) | copy-start | bytes 1572868
  67.5 1.5 %copy-start.4 = (f32[128]{0:T(128)S(1)}, f32[128]{0:T(128)}, u32[]{:S(2)}) copy-start(f32[128]{0:T(128)} %param.18) | copy-start | bytes 1540
Sparse Core Ops, SparseCore 0:
  8.9 60.9 all-gather.1
where the time goes:
time: 131 us; the launch traced here: 130 us
  waiting for transfers between devices  38.2 us (29%)
  matrix products  17.1 us (13%)
  blocking collectives  16.4 us (13%)
  local copies, waits for them, and re-layouts  14.6 us (11%)
  starting transfers between devices  14.1 us (11%)
  between operations  13.6 us (10%)
  other arithmetic  8.36 us (6%)
  loops' own time  7.96 us (6%)
    all_to_all x1, blocking collectives, local(): lax.all_to_all(outputs, 'sp', split_axis=1, concat_axis=2, tiled=True)  16.4 us
    all_to_all x1, waiting for transfers between devices, local(): lax.all_to_all(by_peer(key_rows), 'sp', split_axis=2, concat_axis=1, tile...  13.5 us
    all_to_all x1, waiting for transfers between devices, local(): lax.all_to_all(by_peer(query_rows), 'sp', split_axis=2, concat_axis=1, ti...  12.7 us
    all_to_all x1, waiting for transfers between devices, local(): lax.all_to_all(by_peer(value_rows), 'sp', split_axis=2, concat_axis=1, ti...  11.3 us
    another operation x1, loops' own time, local(): outputs = lax.map(per_head, jnp.arange(local_heads, dtype=jnp.int32))  7.96 us
    sub x4, matrix products, one_block(): totals = jnp.sum(jnp.exp(stored - highest[..., None]), axis=-1)  7.85 us
    all_to_all x1, starting transfers between devices, local(): lax.all_to_all(by_peer(key_rows), 'sp', split_axis=2, concat_axis=1, tile...  6.35 us
    dot_general x1, matrix products, local(): jnp.dot(heads_rows, lax.all_gather(out_weight, 'dp', axis=1, tiled=True),...  5.46 us
  transfers between devices with their start and end apart: 4, of which 3 were waited for; matrix products, arithmetic and copies ran while one was open for 26% of the time, Pallas kernels for 0%

commit v1 on v0

v1 whole, which is shorter than its diff:
```python
import functools
import math

import jax
import jax.numpy as jnp
import numpy as np
from jax import lax
from jax.experimental import pallas as pl
from jax.experimental.pallas import tpu as pltpu
from jax.sharding import PartitionSpec as P

EPSILON = 1e-06
OUT_SCALE = 0.8
CORES = 2
CHUNKS = 2
MESH = pl.DeviceIdType.MESH


def rotation_tables(length, head_size):
    half = head_size // 2
    inverse = np.float32(10000.0) ** (-np.arange(half, dtype=np.float32) / np.float32(half))
    angles = np.arange(length, dtype=np.float32)[:, None] * inverse.astype(np.float32)[None, :]
    cosine, sine = np.cos(angles), np.sin(angles)
    return (
        np.concatenate([cosine] * 4, axis=1).astype(np.float32),
        np.concatenate([-sine, sine] * 2, axis=1).astype(np.float32),
    )


def kernel(
    n, n_dp, head_size, q_ref, k_ref, v_ref, qg_ref, kg_ref, lam_ref, hg_ref, w_ref, cos_ref, sin_ref,
    out_ref, rx, rot_q, rot_k, heads_out, hrx, wfull,
    in_send, in_recv, ret_send, ret_recv, wx_send, wx_recv, wc_send, wc_recv, own_sem,
):
    me = lax.axis_index("sp")
    dp = lax.axis_index("dp")
    cores = CORES if n_dp % CORES == 0 else 1
    nx = n_dp // cores
    xi, core = dp // cores, lax.rem(dp, cores)
    tok = q_ref.shape[1]
    width = 2 * head_size
    local_heads = rx.shape[1]
    length = rx.shape[2]
    depth = w_ref.shape[0]
    cols = w_ref.shape[1]
    piece = depth // CHUNKS

    def sp_peer(off):
        return lax.rem(me + off, n)

    def dp_index(xo, co):
        return lax.rem(xi + xo, nx) * cores + lax.rem(core + co, cores)

    barrier = pltpu.get_barrier_semaphore()
    for off in range(1, n):
        pl.semaphore_signal(barrier, inc=1, device_id={"sp": sp_peer(off)}, device_id_type=MESH)
    for xo in range(1, nx):
        pl.semaphore_signal(barrier, inc=1, device_id={"dp": dp_index(xo, 0)}, device_id_type=MESH)
    for co in range(1, cores):
        pl.semaphore_signal(barrier, inc=1, device_id={"dp": dp_index(0, co)}, device_id_type=MESH)

    sources = (k_ref, q_ref, v_ref)

    def own_rows(t, j):
        column = pl.multiple_of((me * local_heads + j) * width, width)
        return pltpu.make_async_copy(
            sources[t].at[0, :, pl.ds(column, width)],
            rx.at[t, j, pl.ds(pl.multiple_of(me * tok, tok), tok), :],
            in_recv.at[t, j, 0],
        )

    def rows_to(t, j, off):
        peer = sp_peer(off)
        column = pl.multiple_of((peer * local_heads + j) * width, width)
        return pltpu.make_async_remote_copy(
            src_ref=sources[t].at[0, :, pl.ds(column, width)],
            dst_ref=rx.at[t, j, pl.ds(pl.multiple_of(me * tok, tok), tok), :],
            send_sem=in_send.at[t, j, off],
            recv_sem=in_recv.at[t, j, off],
            device_id={"sp": peer},
            device_id_type=MESH,
        )

    def rows_from(t, j, off):
        peer = lax.rem(me + n - off, n)
        block = rx.at[t, j, pl.ds(pl.multiple_of(peer * tok, tok), tok), :]
        return pltpu.make_async_remote_copy(
            src_ref=block, dst_ref=block, send_sem=in_send.at[t, j, off],
            recv_sem=in_recv.at[t, j, off], device_id={"sp": peer}, device_id_type=MESH,
        )

    def weight_x(xo, r):
        rows = pl.ds(r * piece, piece)
        return pltpu.make_async_remote_copy(
            src_ref=w_ref.at[rows, :], dst_ref=wfull.at[dp, rows, :],
            send_sem=wx_send.at[xo, r], recv_sem=wx_recv.at[xo, r],
            device_id={"dp": dp_index(xo, 0)}, device_id_type=MESH,
        )

    def weight_x_in(xo, r):
        block = wfull.at[dp_index(nx - xo, 0), pl.ds(r * piece, piece), :]
        return pltpu.make_async_remote_copy(
            src_ref=block, dst_ref=block, send_sem=wx_send.at[xo, r], recv_sem=wx_recv.at[xo, r],
            device_id={"dp": dp_index(xo, 0)}, device_id_type=MESH,
        )

    def weight_core(xo, r):
        rows = pl.ds(r * piece, piece)
        target = wfull.at[dp_index(nx - xo, 0), rows, :]
        return pltpu.make_async_remote_copy(
            src_ref=w_ref.at[rows, :] if xo == 0 else target, dst_ref=target,
            send_sem=wc_send.at[xo, r], recv_sem=wc_recv.at[xo, r],
            device_id={"dp": dp_index(0, 1)}, device_id_type=MESH,
        )

    def weight_core_in(xo, r):
        block = wfull.at[dp_index(nx - xo, 1), pl.ds(r * piece, piece), :]
        return pltpu.make_async_remote_copy(
            src_ref=block, dst_ref=block, send_sem=wc_send.at[xo, r], recv_sem=wc_recv.at[xo, r],
            device_id={"dp": dp_index(0, 1)}, device_id_type=MESH,
        )

    own_weight = pltpu.make_async_copy(w_ref, wfull.at[dp], own_sem)
    own_weight.start()
    for j in range(local_heads):
        for t in range(3):
            own_rows(t, j).start()
    pl.semaphore_wait(barrier, (n - 1) + (nx - 1) + (cores - 1))
    for j in range(local_heads):
        for t in range(3):
            for off in range(1, n):
                rows_to(t, j, off).start()
        if j == 0:
            for r in range(CHUNKS):
                for xo in range(1, nx):
                    weight_x(xo, r).start()
            if cores > 1:
                for r in range(CHUNKS):
                    weight_core(0, r).start()

    lane = lax.broadcasted_iota(jnp.int32, (1, width), 1)
    low_map = lane < head_size
    low_half = lax.rem(lane, head_size) < head_size // 2

    def norm_rotate(block, gain):
        x = block.astype(jnp.float32)
        square = x * x
        low = jnp.sum(jnp.where(low_map, square, 0.0), axis=1, keepdims=True)
        high = jnp.sum(jnp.where(low_map, 0.0, square), axis=1, keepdims=True)
        low = lax.rsqrt(low * (1.0 / head_size) + EPSILON)
        high = lax.rsqrt(high * (1.0 / head_size) + EPSILON)
        y = x * jnp.where(low_map, low, high) * gain
        quarter = head_size // 2
        turned = jnp.where(low_half, pltpu.roll(y, width - quarter, 1), pltpu.roll(y, quarter, 1))
        return (y * cos_ref[...] + turned * sin_ref[...]).astype(jnp.bfloat16)

    def heads_to(j, i):
        column = pl.multiple_of((me * local_heads + j) * width, width)
        off = lax.rem(i + n - me, n)
        return pltpu.make_async_remote_copy(
            src_ref=heads_out.at[j, i], dst_ref=hrx.at[:, pl.ds(column, width)],
            send_sem=ret_send.at[j, off], recv_sem=ret_recv.at[j, off],
            device_id={"sp": i}, device_id_type=MESH,
        )

    def heads_from(j, off):
        peer = lax.rem(me + n - off, n)
        column = pl.multiple_of((peer * local_heads + j) * width, width)
        block = hrx.at[:, pl.ds(column, width)]
        return pltpu.make_async_remote_copy(
            src_ref=block, dst_ref=block, send_sem=ret_send.at[j, off],
            recv_sem=ret_recv.at[j, off], device_id={"sp": peer}, device_id_type=MESH,
        )

    groups = math.gcd(n, 4)
    per_group = n // groups
    segment = length // groups
    factor = head_size ** (-0.5) * math.log2(math.e)
    contract = (((1,), (1,)), ((), ()))

    def query_block(j, g, i, lam):
        rows = pl.ds(i * tok, tok) if isinstance(i, int) else pl.ds(pl.multiple_of(i * tok, tok), tok)
        q = rot_q[rows, :]
        zero = jnp.zeros_like(q)
        both = jnp.concatenate([jnp.where(low_map, q, zero), jnp.where(low_map, zero, q)], axis=0)
        start = g * segment
        spans = ([(0, start)] if g else []) + [(start, segment)]
        parts = []
        for first, size in spans:
            scores = lax.dot_general(
                both, rot_k[first : first + size, :], contract, preferred_element_type=jnp.float32
            )
            if first == start:
                shape = (2 * tok, size)
                row = lax.rem(lax.broadcasted_iota(jnp.int32, shape, 0), tok) + i * tok
                column = lax.broadcasted_iota(jnp.int32, shape, 1) + first
                scores = jnp.where(column <= row, scores, -1e30)
            parts.append(scores)
        top = functools.reduce(jnp.maximum, [jnp.max(s, axis=1, keepdims=True) for s in parts])
        parts = [jnp.exp2((s - top) * factor) for s in parts]
        total = functools.reduce(jnp.add, [jnp.sum(e, axis=1, keepdims=True) for e in parts])
        inverse = 1.0 / total
        one, two = inverse[:tok], inverse[tok:] * lam
        raw = None
        for (first, size), e in zip(spans, parts):
            mixing = (e[:tok] * one - e[tok:] * two).astype(jnp.bfloat16)
            term = jnp.dot(mixing, rx[2, j, first : first + size, :], preferred_element_type=jnp.float32)
            raw = term if raw is None else raw + term
        scaled = raw * lax.rsqrt(jnp.mean(raw * raw, axis=1, keepdims=True) + EPSILON)
        result = (scaled * hg_ref[...] * OUT_SCALE).astype(jnp.bfloat16)

        @pl.when(i == me)
        def _():
            column = pl.multiple_of((me * local_heads + j) * width, width)
            hrx[:, pl.ds(column, width)] = result

        @pl.when(i != me)
        def _():
            heads_out[j, i] = result
            heads_to(j, i).start()

    def forward(r):
        if cores > 1:
            for xo in range(1, nx):
                weight_x_in(xo, r).wait_recv()
                weight_core(xo, r).start()

    for j in range(local_heads):
        lam = lam_ref[me * local_heads + j]
        for t, (target, gain) in enumerate(((rot_k, kg_ref), (rot_q, qg_ref), (None, None))):
            own_rows(t, j).wait()
            for off in range(1, n):
                rows_from(t, j, off).wait_recv()
            if target is not None:
                target[...] = norm_rotate(rx[t, j], gain[...])
        for g in range(groups):
            if per_group == 1:
                query_block(j, g, g, lam)
            else:
                def step(b, carry, j=j, g=g, lam=lam):
                    query_block(j, g, g * per_group + b, lam)
                    return carry
                lax.fori_loop(0, per_group, step, 0)
        if j == max(local_heads - 2, 0):
            forward(0)
    for r in range(1, CHUNKS):
        forward(r)

    for j in range(local_heads):
        for off in range(1, n):
            heads_from(j, off).wait_recv()
    own_weight.wait()
    rows = hrx[...]

    def project(index):
        column = pl.multiple_of(index * cols, cols)
        out_ref[0, :, pl.ds(column, cols)] = jnp.dot(
            rows, wfull[index], preferred_element_type=jnp.float32
        ).astype(out_ref.dtype)

    for co in range(cores):
        for xo in range(nx):
            for r in range(CHUNKS):
                if co:
                    weight_core_in(xo, r).wait_recv()
                elif xo and cores == 1:
                    weight_x_in(xo, r).wait_recv()
            project(dp_index(nx - xo, co))

    for j in range(local_heads):
        for off in range(1, n):
            for t in range(3):
                rows_to(t, j, off).wait_send()
            heads_to(j, sp_peer(off)).wait_send()
    for r in range(CHUNKS):
        for xo in range(nx):
            if xo:
                weight_x(xo, r).wait_send()
            if cores > 1:
                weight_core(xo, r).wait_send()


def local(n, n_dp, query_rows, key_rows, value_rows, query_gain, key_gain, lambdas, head_gain, out_weight):
    tok = query_rows.shape[1]
    head_size = query_gain.shape[0]
    width = head_gain.shape[0]
    local_heads = lambdas.shape[0] // n
    length = tok * n
    depth, cols = out_weight.shape
    cores = CORES if n_dp % CORES == 0 else 1
    nx = n_dp // cores
    cosine, sine = rotation_tables(length, head_size)
    anywhere = pl.BlockSpec(memory_space=pl.ANY)
    vmem = pl.BlockSpec(memory_space=pltpu.VMEM)
    dma = pltpu.SemaphoreType.DMA
    return pl.pallas_call(
        functools.partial(kernel, n, n_dp, head_size),
        out_shape=jax.ShapeDtypeStruct((1, tok, n_dp * cols), jnp.bfloat16),
        in_specs=[anywhere] * 3
        + [vmem, vmem, pl.BlockSpec(memory_space=pltpu.SMEM), vmem, anywhere, vmem, vmem],
        out_specs=vmem,
        scratch_shapes=[
            pltpu.VMEM((3, local_heads, length, width), jnp.bfloat16),
            pltpu.VMEM((length, width), jnp.bfloat16),
            pltpu.VMEM((length, width), jnp.bfloat16),
            pltpu.VMEM((local_heads, n, tok, width), jnp.bfloat16),
            pltpu.VMEM((tok, depth), jnp.bfloat16),
            pltpu.VMEM((n_dp, depth, cols), jnp.bfloat16),
            dma((3, local_heads, n)),
            dma((3, local_heads, n)),
            dma((local_heads, n)),
            dma((local_heads, n)),
            dma((nx, CHUNKS)),
            dma((nx, CHUNKS)),
            dma((nx, CHUNKS)),
            dma((nx, CHUNKS)),
            dma(()),
        ],
        compiler_params=pltpu.CompilerParams(
            collective_id=0, has_side_effects=True, vmem_limit_bytes=56 * 1024 * 1024
        ),
    )(
        query_rows, key_rows, value_rows,
        jnp.tile(query_gain, 2)[None, :], jnp.tile(key_gain, 2)[None, :], lambdas, head_gain[None, :],
        out_weight, jnp.asarray(cosine), jnp.asarray(sine),
    )


def solution(mesh):
    rows = P(("grp", "dp"), "sp", None)
    return jax.shard_map(
        functools.partial(local, mesh.shape["sp"], mesh.shape["dp"]),
        mesh=mesh,
        in_specs=(rows, rows, rows, P(), P(), P(), P(), P(None, "dp")),
        out_specs=rows,
        check_vma=False,
    )
```

time: 131 us -> 62.7 us (0.48)
  Pallas kernels: 0 us -> 57.6 us
  waiting for transfers between devices: 38.2 us -> 0 us
  matrix products: 17.1 us -> 0 us
  blocking collectives: 16.4 us -> 0 us
  starting transfers between devices: 14.1 us -> 0 us
  between operations: 13.6 us -> 0.01 us
  local copies, waits for them, and re-layouts: 14.6 us -> 4.46 us
  other arithmetic: 8.36 us -> 0 us
  loops' own time: 7.96 us -> 0 us
    pallas_call x0 -> x1, Pallas kernels: none -> 57.6 us  [local(): pl.pallas_call(functools.partial(kernel, n, n_dp, head_size), out_shape=j...]
    all_to_all x3 -> x0, waiting for transfers between devices: 37.5 us -> none  [the longest x1 13.5 us: local(): lax.all_to_all(by_peer(key_rows), 'sp', split_axis=2, concat_axis=1, tile...]
    all_to_all x1 -> x0, blocking collectives: 16.4 us -> none  [local(): lax.all_to_all(outputs, 'sp', split_axis=1, concat_axis=2, tiled=True)]
    all_to_all x3 -> x0, starting transfers between devices: 14.1 us -> none  [the longest x1 6.35 us: local(): lax.all_to_all(by_peer(key_rows), 'sp', split_axis=2, concat_axis=1, tile...]
    dot_general x5 -> x0, matrix products: 9.23 us -> none  [the longest x1 5.46 us: local(): jnp.dot(heads_rows, lax.all_gather(out_weight, 'dp', axis=1, tiled=True),...]
    another operation x1 -> x0, loops' own time: 7.96 us -> none  [local(): outputs = lax.map(per_head, jnp.arange(local_heads, dtype=jnp.int32))]
    sub x4 -> x0, matrix products: 7.85 us -> none  [one_block(): totals = jnp.sum(jnp.exp(stored - highest[..., None]), axis=-1)]
    dynamic_slice x9 -> x0, local copies, waits for them, and re-layouts: 4.78 us -> none  [the longest x4 2.36 us: per_head(): local_lambdas[head_index]]
  transfers between devices with their start and end apart: 4 -> 0, of which waited for: 3 -> 0; matrix products, arithmetic and copies ran while one was open for 26% -> 0% of each run, Pallas kernels for 0% -> 0%
where the time goes in v1:
time: 62.7 us; the launch traced here: 62.1 us
  Pallas kernels  57.6 us (92%)
  local copies, waits for them, and re-layouts  4.46 us (7%)
    pallas_call x1, Pallas kernels, local(): pl.pallas_call(functools.partial(kernel, n, n_dp, head_size), out_shape=j...  57.6 us
    unnamed x1, local copies, waits for them, and re-layouts  1.88 us
    another operation x2, local copies, waits for them, and re-layouts, local(): jnp.tile(key_gain, 2)[None, :]  1.33 us

profile of v1, /device:TPU:0, one launch (start us, length us, event | category | flops | bytes accessed | tf_op | source)
XLA Modules:
  0.0 62.1 jit_solution(14915689279070013531)
XLA Ops:
  0.0 0.7 %tile.4 = f32[2,64]{1,0:T(2,128)S(1)} broadcast(f32[64]{0:T(128)} %param.13), dimensions={1} | broadcast | bytes 768 | tf_op jit(solution)/shard_map/tile | solution.py:324
  0.7 0.6 broadcast_in_dim_tile.6.qg_ref
  1.2 0.7 %tile.5 = f32[2,64]{1,0:T(2,128)S(1)} broadcast(f32[64]{0:T(128)} %param.14), dimensions={1} | broadcast | bytes 768 | tf_op jit(solution)/shard_map/tile | solution.py:324
  1.9 0.7 %broadcast_in_dim_tile.7.kg_ref = f32[1,128]{1,0:T(1,128)} reshape(f32[2,64]{1,0:T(2,128)S(1)} %tile.5) | data formatting | bytes 1024 | tf_op jit(solution)/shard_map/broadcast_in_dim;tile | solution.py:324
  2.6 57.6 %shard_map.100 = bf16[1,128,2048]{2,1,0:T(8,128)(2,1)} custom-call(bf16[1,128,2048]{2,1,0:T(8,128)(2,1)} %q_ref.1, bf16[1,128,2048]{2,1,0:T(8,128)(2,1)} %k_ref.1, bf16[1,128,2048]{2,1,0:T(8,128)(2,1)} %v_ref.1, f32[1,128]{1,0:T(1,128)} %broadcast_in_dim_tile.6.qg_ref, f32[1,128]{1,0:T(1,128)} %broadcast_in_dim_tile.7.kg_ref, f32[16]{0:T(128)} %lam_ref.1, ...), custom_call_target="tpu_custom_call" | custom-call | tf_op jit(solution)/shard_map/pallas_call | solution.py:296
  60.2 1.9 %copy.12 = bf16[1,128,2048]{2,1,0:T(8,128)(2,1)} copy(bf16[1,128,2048]{2,1,0:T(8,128)(2,1)} %shard_map.100) | data formatting | bytes 1048576

commit v2 on v1

--- a/solution.py
+++ b/solution.py
@@ -13,6 +13,7 @@
 OUT_SCALE = 0.8
 CORES = 2
 CHUNKS = 2
+WAYS = 2
 MESH = pl.DeviceIdType.MESH
 
 
@@ -28,12 +29,14 @@
 
 
 def kernel(
-    n, n_dp, head_size, q_ref, k_ref, v_ref, qg_ref, kg_ref, lam_ref, hg_ref, w_ref, cos_ref, sin_ref,
-    out_ref, rx, rot_q, rot_k, heads_out, hrx, wfull,
-    in_send, in_recv, ret_send, ret_recv, wx_send, wx_recv, wc_send, wc_recv, own_sem,
+    n, n_dp, n_grp, head_size, q_ref, k_ref, v_ref, qg_ref, kg_ref, lam_ref, hg_ref, w_ref, cos_ref, sin_ref,
+    out_ref, total, rx, rot_q, rot_k, heads_out, hrx, wfull,
+    in_send, in_recv, ret_send, ret_recv, wx_send, wx_recv, wy_send, wy_recv, wc_send, wc_recv, own_sem,
 ):
     me = lax.axis_index("sp")
     dp = lax.axis_index("dp")
+    ways = WAYS if n_grp == WAYS else 1
+    grp = lax.axis_index("grp") if ways > 1 else 0
     cores = CORES if n_dp % CORES == 0 else 1
     nx = n_dp // cores
     xi, core = dp // cores, lax.rem(dp, cores)
@@ -43,7 +46,7 @@
     length = rx.shape[2]
     depth = w_ref.shape[0]
     cols = w_ref.shape[1]
-    piece = depth // CHUNKS
+    piece = depth // (CHUNKS * ways)
 
     def sp_peer(off):
         return lax.rem(me + off, n)
@@ -59,6 +62,11 @@
     for co in range(1, cores):
         pl.semaphore_signal(barrier, inc=1, device_id={"dp": dp_index(0, co)}, device_id_type=MESH)
 
+    if ways > 1:
+        pl.semaphore_signal(
+            barrier, inc=1, device_id={"grp": lax.rem(grp + 1, ways)}, device_id_type=MESH
+        )
+
     sources = (k_ref, q_ref, v_ref)
 
     def own_rows(t, j):
@@ -89,35 +97,47 @@
             recv_sem=in_recv.at[t, j, off], device_id={"sp": peer}, device_id_type=MESH,
         )
 
+    def piece_rows(r, way):
+        first = (r * ways + lax.rem(grp + way, ways)) * piece
+        return pl.ds(pl.multiple_of(first, piece), piece)
+
+    def moved(source, target, send_sem, recv_sem, device):
+        return pltpu.make_async_remote_copy(
+            src_ref=source, dst_ref=target, send_sem=send_sem, recv_sem=recv_sem,
+            device_id=device, device_id_type=MESH,
+        )
+
     def weight_x(xo, r):
-        rows = pl.ds(r * piece, piece)
-        return pltpu.make_async_remote_copy(
-            src_ref=w_ref.at[rows, :], dst_ref=wfull.at[dp, rows, :],
-            send_sem=wx_send.at[xo, r], recv_sem=wx_recv.at[xo, r],
-            device_id={"dp": dp_index(xo, 0)}, device_id_type=MESH,
+        rows = piece_rows(r, 0)
+        return moved(
+            w_ref.at[rows, :], wfull.at[dp, rows, :], wx_send.at[xo, r], wx_recv.at[xo, r],
+            {"dp": dp_index(xo, 0)},
         )
 
     def weight_x_in(xo, r):
-        block = wfull.at[dp_index(nx - xo, 0), pl.ds(r * piece, piece), :]
-        return pltpu.make_async_remote_copy(
-            src_ref=block, dst_ref=block, send_sem=wx_send.at[xo, r], recv_sem=wx_recv.at[xo, r],
-            device_id={"dp": dp_index(xo, 0)}, device_id_type=MESH,
-        )
-
-    def weight_core(xo, r):
-        rows = pl.ds(r * piece, piece)
+        block = wfull.at[dp_index(nx - xo, 0), piece_rows(r, 0), :]
+        return moved(block, block, wx_send.at[xo, r], wx_recv.at[xo, r], {"dp": dp_index(xo, 0)})
+
+    def weight_y(xo, r):
+        block = wfull.at[dp_index(nx - xo, 0), piece_rows(r, 0), :]
+        return moved(block, block, wy_send.at[xo, r], wy_recv.at[xo, r], {"grp": lax.rem(grp + 1, ways)})
+
+    def weight_y_in(xo, r):
+        block = wfull.at[dp_index(nx - xo, 0), piece_rows(r, 1), :]
+        return moved(block, block, wy_send.at[xo, r], wy_recv.at[xo, r], {"grp": lax.rem(grp + 1, ways)})
+
+    def weight_core(xo, r, way):
+        rows = piece_rows(r, way)
         target = wfull.at[dp_index(nx - xo, 0), rows, :]
-        return pltpu.make_async_remote_copy(
-            src_ref=w_ref.at[rows, :] if xo == 0 else target, dst_ref=target,
-            send_sem=wc_send.at[xo, r], recv_sem=wc_recv.at[xo, r],
-            device_id={"dp": dp_index(0, 1)}, device_id_type=MESH,
-        )
-
-    def weight_core_in(xo, r):
-        block = wfull.at[dp_index(nx - xo, 1), pl.ds(r * piece, piece), :]
-        return pltpu.make_async_remote_copy(
-            src_ref=block, dst_ref=block, send_sem=wc_send.at[xo, r], recv_sem=wc_recv.at[xo, r],
-            device_id={"dp": dp_index(0, 1)}, device_id_type=MESH,
+        return moved(
+            w_ref.at[rows, :] if xo == 0 else target, target,
+            wc_send.at[xo, r, way], wc_recv.at[xo, r, way], {"dp": dp_index(0, 1)},
+        )
+
+    def weight_core_in(xo, r, way):
+        block = wfull.at[dp_index(nx - xo, 1), piece_rows(r, way), :]
+        return moved(
+            block, block, wc_send.at[xo, r, way], wc_recv.at[xo, r, way], {"dp": dp_index(0, 1)}
         )
 
     own_weight = pltpu.make_async_copy(w_ref, wfull.at[dp], own_sem)
@@ -125,7 +145,7 @@
     for j in range(local_heads):
         for t in range(3):
             own_rows(t, j).start()
-    pl.semaphore_wait(barrier, (n - 1) + (nx - 1) + (cores - 1))
+    pl.semaphore_wait(barrier, (n - 1) + (nx - 1) + (cores - 1) + (ways - 1))
     for j in range(local_heads):
         for t in range(3):
             for off in range(1, n):
@@ -136,7 +156,8 @@
                     weight_x(xo, r).start()
             if cores > 1:
                 for r in range(CHUNKS):
-                    weight_core(0, r).start()
+                    for way in range(ways):
+                        weight_core(0, r, way).start()
 
     lane = lax.broadcasted_iota(jnp.int32, (1, width), 1)
     low_map = lane < head_size
@@ -155,18 +176,18 @@
         return (y * cos_ref[...] + turned * sin_ref[...]).astype(jnp.bfloat16)
 
     def heads_to(j, i):
-        column = pl.multiple_of((me * local_heads + j) * width, width)
+        column = pl.multiple_of(me * width, width)
         off = lax.rem(i + n - me, n)
         return pltpu.make_async_remote_copy(
-            src_ref=heads_out.at[j, i], dst_ref=hrx.at[:, pl.ds(column, width)],
+            src_ref=heads_out.at[j, i], dst_ref=hrx.at[j, :, pl.ds(column, width)],
             send_sem=ret_send.at[j, off], recv_sem=ret_recv.at[j, off],
             device_id={"sp": i}, device_id_type=MESH,
         )
 
     def heads_from(j, off):
         peer = lax.rem(me + n - off, n)
-        column = pl.multiple_of((peer * local_heads + j) * width, width)
-        block = hrx.at[:, pl.ds(column, width)]
+        column = pl.multiple_of(peer * width, width)
+        block = hrx.at[j, :, pl.ds(column, width)]
         return pltpu.make_async_remote_copy(
             src_ref=block, dst_ref=block, send_sem=ret_send.at[j, off],
             recv_sem=ret_recv.at[j, off], device_id={"sp": peer}, device_id_type=MESH,
@@ -211,19 +232,26 @@
 
         @pl.when(i == me)
         def _():
-            column = pl.multiple_of((me * local_heads + j) * width, width)
-            hrx[:, pl.ds(column, width)] = result
+            hrx[j, :, pl.ds(pl.multiple_of(me * width, width), width)] = result
 
         @pl.when(i != me)
         def _():
             heads_out[j, i] = result
             heads_to(j, i).start()
 
-    def forward(r):
-        if cores > 1:
+    def forward(stage):
+        if stage < CHUNKS:
             for xo in range(1, nx):
-                weight_x_in(xo, r).wait_recv()
-                weight_core(xo, r).start()
+                weight_x_in(xo, stage).wait_recv()
+                if ways > 1:
+                    weight_y(xo, stage).start()
+                if cores > 1:
+                    weight_core(xo, stage, 0).start()
+        elif ways > 1:
+            for xo in range(1, nx):
+                weight_y_in(xo, stage - CHUNKS).wait_recv()
+                if cores > 1:
+                    weight_core(xo, stage - CHUNKS, 1).start()
 
     for j in range(local_heads):
         lam = lam_ref[me * local_heads + j]
@@ -241,31 +269,33 @@
                     query_block(j, g, g * per_group + b, lam)
                     return carry
                 lax.fori_loop(0, per_group, step, 0)
-        if j == max(local_heads - 2, 0):
-            forward(0)
-    for r in range(1, CHUNKS):
-        forward(r)
+        for stage in range(2 * CHUNKS):
+            if j == min(stage, local_heads - 1):
+                forward(stage)
+
+    own_weight.wait()
+    if cores > 1:
+        for xo in range(nx):
+            for r in range(CHUNKS):
+                for way in range(ways):
+                    weight_core_in(xo, r, way).wait_recv()
 
     for j in range(local_heads):
         for off in range(1, n):
             heads_from(j, off).wait_recv()
-    own_weight.wait()
-    rows = hrx[...]
-
-    def project(index):
-        column = pl.multiple_of(index * cols, cols)
-        out_ref[0, :, pl.ds(column, cols)] = jnp.dot(
-            rows, wfull[index], preferred_element_type=jnp.float32
-        ).astype(out_ref.dtype)
-
-    for co in range(cores):
-        for xo in range(nx):
-            for r in range(CHUNKS):
-                if co:
-                    weight_core_in(xo, r).wait_recv()
-                elif xo and cores == 1:
-                    weight_x_in(xo, r).wait_recv()
-            project(dp_index(nx - xo, co))
+        rows = hrx[j]
+        for index in range(n_dp):
+            matching = jnp.concatenate(
+                [wfull[index, pl.ds((s * local_heads + j) * width, width), :] for s in range(n)], axis=0
+            )
+            term = jnp.dot(rows, matching, preferred_element_type=jnp.float32)
+            span = slice(index * cols, (index + 1) * cols)
+            if j:
+                term = total[:, span] + term
+            if j == local_heads - 1:
+                out_ref[0, :, span] = term.astype(out_ref.dtype)
+            else:
+                total[:, span] = term
 
     for j in range(local_heads):
         for off in range(1, n):
@@ -276,11 +306,14 @@
         for xo in range(nx):
             if xo:
                 weight_x(xo, r).wait_send()
+                if ways > 1:
+                    weight_y(xo, r).wait_send()
             if cores > 1:
-                weight_core(xo, r).wait_send()
-
-
-def local(n, n_dp, query_rows, key_rows, value_rows, query_gain, key_gain, lambdas, head_gain, out_weight):
+                for way in range(ways):
+                    weight_core(xo, r, way).wait_send()
+
+
+def local(n, n_dp, n_grp, query_rows, key_rows, value_rows, query_gain, key_gain, lambdas, head_gain, out_weight):
     tok = query_rows.shape[1]
     head_size = query_gain.shape[0]
     width = head_gain.shape[0]
@@ -294,17 +327,18 @@
     vmem = pl.BlockSpec(memory_space=pltpu.VMEM)
     dma = pltpu.SemaphoreType.DMA
     return pl.pallas_call(
-        functools.partial(kernel, n, n_dp, head_size),
+        functools.partial(kernel, n, n_dp, n_grp, head_size),
         out_shape=jax.ShapeDtypeStruct((1, tok, n_dp * cols), jnp.bfloat16),
         in_specs=[anywhere] * 3
         + [vmem, vmem, pl.BlockSpec(memory_space=pltpu.SMEM), vmem, anywhere, vmem, vmem],
         out_specs=vmem,
         scratch_shapes=[
+            pltpu.VMEM((tok, n_dp * cols), jnp.float32),
             pltpu.VMEM((3, local_heads, length, width), jnp.bfloat16),
             pltpu.VMEM((length, width), jnp.bfloat16),
             pltpu.VMEM((length, width), jnp.bfloat16),
             pltpu.VMEM((local_heads, n, tok, width), jnp.bfloat16),
-            pltpu.VMEM((tok, depth), jnp.bfloat16),
+            pltpu.VMEM((local_heads, tok, n * width), jnp.bfloat16),
             pltpu.VMEM((n_dp, depth, cols), jnp.bfloat16),
             dma((3, local_heads, n)),
             dma((3, local_heads, n)),
@@ -314,6 +348,8 @@
             dma((nx, CHUNKS)),
             dma((nx, CHUNKS)),
             dma((nx, CHUNKS)),
+            dma((nx, CHUNKS, WAYS)),
+            dma((nx, CHUNKS, WAYS)),
             dma(()),
         ],
         compiler_params=pltpu.CompilerParams(
@@ -329,7 +365,7 @@
 def solution(mesh):
     rows = P(("grp", "dp"), "sp", None)
     return jax.shard_map(
-        functools.partial(local, mesh.shape["sp"], mesh.shape["dp"]),
+        functools.partial(local, mesh.shape["sp"], mesh.shape["dp"], mesh.shape["grp"]),
         mesh=mesh,
         in_specs=(rows, rows, rows, P(), P(), P(), P(), P(None, "dp")),
         out_specs=rows,

time: 62.7 us -> 59.5 us (0.949)
  Pallas kernels: 57.6 us -> 54.8 us
    pallas_call x1, Pallas kernels: 57.6 us -> 54.8 us  [local(): pl.pallas_call(functools.partial(kernel, n, n_dp, n_grp, head_size), out_...]
where the time goes in v2:
time: 59.5 us; the launch traced here: 59.3 us
  Pallas kernels  54.8 us (92%)
  local copies, waits for them, and re-layouts  4.46 us (7%)
    pallas_call x1, Pallas kernels, local(): pl.pallas_call(functools.partial(kernel, n, n_dp, n_grp, head_size), out_...  54.8 us
    unnamed x1, local copies, waits for them, and re-layouts  1.88 us
    another operation x2, local copies, waits for them, and re-layouts, local(): jnp.tile(key_gain, 2)[None, :]  1.33 us
    another operation x2, local copies, waits for them, and re-layouts, local(): jnp.tile(query_gain, 2)[None, :]  1.25 us

profile of v2, /device:TPU:0, one launch (start us, length us, event | category | flops | bytes accessed | tf_op | source)
XLA Modules:
  0.0 59.3 jit_solution(1732928861374188942)
XLA Ops:
  0.0 0.7 %tile.4 = f32[2,64]{1,0:T(2,128)S(1)} broadcast(f32[64]{0:T(128)} %param.13), dimensions={1} | broadcast | bytes 768 | tf_op jit(solution)/shard_map/tile | solution.py:360
  0.7 0.6 broadcast_in_dim_tile.6.qg_ref
  1.2 0.7 %tile.5 = f32[2,64]{1,0:T(2,128)S(1)} broadcast(f32[64]{0:T(128)} %param.14), dimensions={1} | broadcast | bytes 768 | tf_op jit(solution)/shard_map/tile | solution.py:360
  1.9 0.7 %broadcast_in_dim_tile.7.kg_ref = f32[1,128]{1,0:T(1,128)} reshape(f32[2,64]{1,0:T(2,128)S(1)} %tile.5) | data formatting | bytes 1024 | tf_op jit(solution)/shard_map/broadcast_in_dim;tile | solution.py:360
  2.6 54.8 %shard_map.100 = bf16[1,128,2048]{2,1,0:T(8,128)(2,1)} custom-call(bf16[1,128,2048]{2,1,0:T(8,128)(2,1)} %q_ref.1, bf16[1,128,2048]{2,1,0:T(8,128)(2,1)} %k_ref.1, bf16[1,128,2048]{2,1,0:T(8,128)(2,1)} %v_ref.1, f32[1,128]{1,0:T(1,128)} %broadcast_in_dim_tile.6.qg_ref, f32[1,128]{1,0:T(1,128)} %broadcast_in_dim_tile.7.kg_ref, f32[16]{0:T(128)} %lam_ref.1, ...), custom_call_target="tpu_custom_call" | custom-call | tf_op jit(solution)/shard_map/pallas_call | solution.py:329
  57.4 1.9 %copy.12 = bf16[1,128,2048]{2,1,0:T(8,128)(2,1)} copy(bf16[1,128,2048]{2,1,0:T(8,128)(2,1)} %shard_map.100) | data formatting | bytes 1048576

commit v3 on v2

--- a/solution.py
+++ b/solution.py
@@ -29,9 +29,9 @@
 
 
 def kernel(
-    n, n_dp, n_grp, head_size, q_ref, k_ref, v_ref, qg_ref, kg_ref, lam_ref, hg_ref, w_ref, cos_ref, sin_ref,
+    n, n_dp, n_grp, head_size, q_ref, k_ref, v_ref, qg_ref, kg_ref, lam_ref, hg_ref, w_ref, cos_in, sin_in,
     out_ref, total, rx, rot_q, rot_k, heads_out, hrx, wfull,
-    in_send, in_recv, ret_send, ret_recv, wx_send, wx_recv, wy_send, wy_recv, wc_send, wc_recv, own_sem,
+    in_send, in_recv, ret_send, ret_recv, wx_send, wx_recv, wy_send, wy_recv, wc_send, wc_recv, own_sem, cos_ref, sin_ref, table_sem,
 ):
     me = lax.axis_index("sp")
     dp = lax.axis_index("dp")
@@ -142,6 +142,12 @@
 
     own_weight = pltpu.make_async_copy(w_ref, wfull.at[dp], own_sem)
     own_weight.start()
+    tables = [
+        pltpu.make_async_copy(cos_in, cos_ref, table_sem.at[0]),
+        pltpu.make_async_copy(sin_in, sin_ref, table_sem.at[1]),
+    ]
+    for table in tables:
+        table.start()
     for j in range(local_heads):
         for t in range(3):
             own_rows(t, j).start()
@@ -253,6 +259,8 @@
                 if cores > 1:
                     weight_core(xo, stage - CHUNKS, 1).start()
 
+    for table in tables:
+        table.wait()
     for j in range(local_heads):
         lam = lam_ref[me * local_heads + j]
         for t, (target, gain) in enumerate(((rot_k, kg_ref), (rot_q, qg_ref), (None, None))):
@@ -260,7 +268,7 @@
             for off in range(1, n):
                 rows_from(t, j, off).wait_recv()
             if target is not None:
-                target[...] = norm_rotate(rx[t, j], gain[...])
+                target[...] = norm_rotate(rx[t, j], jnp.concatenate([gain[...]] * 2, axis=1))
         for g in range(groups):
             if per_group == 1:
                 query_block(j, g, g, lam)
@@ -330,7 +338,7 @@
         functools.partial(kernel, n, n_dp, n_grp, head_size),
         out_shape=jax.ShapeDtypeStruct((1, tok, n_dp * cols), jnp.bfloat16),
         in_specs=[anywhere] * 3
-        + [vmem, vmem, pl.BlockSpec(memory_space=pltpu.SMEM), vmem, anywhere, vmem, vmem],
+        + [vmem, vmem, pl.BlockSpec(memory_space=pltpu.SMEM), vmem, anywhere, anywhere, anywhere],
         out_specs=vmem,
         scratch_shapes=[
             pltpu.VMEM((tok, n_dp * cols), jnp.float32),
@@ -351,13 +359,16 @@
             dma((nx, CHUNKS, WAYS)),
             dma((nx, CHUNKS, WAYS)),
             dma(()),
+            pltpu.VMEM((length, width), jnp.float32),
+            pltpu.VMEM((length, width), jnp.float32),
+            dma((2,)),
         ],
         compiler_params=pltpu.CompilerParams(
             collective_id=0, has_side_effects=True, vmem_limit_bytes=56 * 1024 * 1024
         ),
     )(
         query_rows, key_rows, value_rows,
-        jnp.tile(query_gain, 2)[None, :], jnp.tile(key_gain, 2)[None, :], lambdas, head_gain[None, :],
+        query_gain[None, :], key_gain[None, :], lambdas, head_gain[None, :],
         out_weight, jnp.asarray(cosine), jnp.asarray(sine),
     )
 

time: 59.5 us -> 56.6 us (0.951)
  local copies, waits for them, and re-layouts: 4.46 us -> 1.88 us
    another operation x4 -> x0, local copies, waits for them, and re-layouts: 2.58 us -> none  [the longest x2 1.33 us: local(): jnp.tile(key_gain, 2)[None, :]]
where the time goes in v3:
time: 56.6 us; the launch traced here: 56.4 us
  Pallas kernels  54.6 us (96%)
  local copies, waits for them, and re-layouts  1.88 us (3%)
    pallas_call x1, Pallas kernels, local(): pl.pallas_call(functools.partial(kernel, n, n_dp, n_grp, head_size), out_...  54.6 us
    unnamed x1, local copies, waits for them, and re-layouts  1.88 us

profile of v3, /device:TPU:0, one launch (start us, length us, event | category | flops | bytes accessed | tf_op | source)
XLA Modules:
  0.0 56.4 jit_solution(15447624880903575897)
XLA Ops:
  0.0 54.6 %shard_map.100 = bf16[1,128,2048]{2,1,0:T(8,128)(2,1)} custom-call(bf16[1,128,2048]{2,1,0:T(8,128)(2,1)} %q_ref.1, bf16[1,128,2048]{2,1,0:T(8,128)(2,1)} %k_ref.1, bf16[1,128,2048]{2,1,0:T(8,128)(2,1)} %v_ref.1, f32[1,64]{1,0:T(1,128)} %bitcast.3, f32[1,64]{1,0:T(1,128)} %bitcast.4, f32[16]{0:T(128)} %lam_ref.1, f32[1,128]{1,0:T(1,128)} %bitcast.5, ...), custom_call_target="tpu_custom_call" | custom-call | tf_op jit(solution)/shard_map/pallas_call | solution.py:337
  54.6 1.9 %copy.12 = bf16[1,128,2048]{2,1,0:T(8,128)(2,1)} copy(bf16[1,128,2048]{2,1,0:T(8,128)(2,1)} %shard_map.100) | data formatting | bytes 1048576
